TPU v7x, 32 devices: a whole 2x2x4 slice. The times are simulated.
32 devices in a mesh: dp: 4 (over y, x), kv: 4 (over z), tp: 2 (over core).
Axes of the slice: x: 2, y: 2, z: 4, core: 2. Of those that a mesh axis runs over, the one named last changes fastest.
Arguments:
- tokens: bfloat16 [16, 16, 2048], P('dp', None, 'kv'), may hold values from -6 to 6
- norm_gain: float32 [2048], P('kv'), may hold values from 0.1 to 1.9
- w_query: bfloat16 [2048, 1024], P('kv', 'tp'), may hold values from -0.125 to 0.125
- w_key: bfloat16 [2048, 1024], P('kv', 'tp'), may hold values from -0.125 to 0.125
- w_value: bfloat16 [2048, 1024], P('kv', 'tp'), may hold values from -0.125 to 0.125
- w_forget: bfloat16 [2048, 16], replicated, may hold values from -0.125 to 0.125
- forget_bias: float32 [16], replicated, may hold values from -2 to 4
- query_gain: float32 [64], replicated, may hold values from 0.1 to 1.9
- key_gain: float32 [64], replicated, may hold values from 0.1 to 1.9
- head_gain: float32 [64], replicated, may hold values from 0.1 to 1.9
- w_out: bfloat16 [1024, 2048], P('tp', 'kv'), may hold values from -0.1875 to 0.1875
- key_cache: bfloat16 [16, 2048, 1024], P('dp', 'kv', 'tp'), may hold values from -240 to 240
- value_cache: bfloat16 [16, 2048, 1024], P('dp', 'kv', 'tp'), may hold values from -6 to 6
- gate_cache: float32 [16, 16, 2048], P('dp', 'tp', 'kv'), may hold values from -242 to 0, as said below
- lengths: int32 [16], P('dp'), may hold values from 1005 to 2028
- accepted: int32 [16], P('dp'), may hold values from 0 to 4
- parents: int32 [16, 16], P('dp'), may hold values from -1 to 14, as said below
Outputs:
- layer_out: bfloat16 [16, 16, 2048], P('dp', None, 'kv')
- new_keys: bfloat16 [16, 2048, 1024], P('dp', 'kv', 'tp')
- new_values: bfloat16 [16, 2048, 1024], P('dp', 'kv', 'tp')
- proposal_gates: float32 [16, 16, 16], P('dp', None, 'tp')
Inputs may be any that keep to these rules, and one draw needn't show every extreme that they name: `gate_cache`: each entry is the running sum of log forget gates up to its position, so entries never rise along positions; entries at and after lengths hold the last step's proposals in order. `parents`: proposal 0 follows the last accepted token (parent -1); every other proposal's parent is one of the three proposals before it.
All inputs are finite; a program needn't handle non-finite values.
Results may differ from a plain program's by a relative error of at most 0.0051.
The roundings to bfloat16 on the way count: a program that leaves them out, or rounds other values in their place, can miss the bound.
Values may be sent and summed in bfloat16 or wider, within the bound.
A program may use at most 64 MiB of HBM per device.

v0:
```python
import jax
import jax.numpy as jnp
from jax import lax
from jax.sharding import PartitionSpec as P

EPSILON = 1e-06
MASKED = -1e30


def head_norm(head_rows, gain_vec):
    mean_square = jnp.mean(head_rows * head_rows, axis=-1, keepdims=True)
    return head_rows * lax.rsqrt(mean_square + EPSILON) * gain_vec


def ancestry(parents):
    count_all = parents.shape[1]
    step_ids = jnp.arange(count_all, dtype=jnp.int32)
    step_matrix = (parents[:, :, None] == step_ids[None, None, :]).astype(jnp.float32)
    identity = jnp.broadcast_to(jnp.eye(count_all, dtype=jnp.float32), step_matrix.shape)

    def extend(turn_index, ancestors):
        return identity + jnp.einsum(
            "sij,sjk->sik", step_matrix, ancestors, precision=lax.Precision.HIGHEST
        )

    return lax.fori_loop(0, count_all, extend, identity)


def combine(earlier, later):
    earlier_max, earlier_total, earlier_sum = earlier
    later_max, later_total, later_sum = later
    row_max = jnp.maximum(earlier_max, later_max)
    earlier_scale = jnp.exp(earlier_max - row_max)
    later_scale = jnp.exp(later_max - row_max)
    spread = earlier_max.shape + (-1,)
    joined = (
        earlier_sum.reshape(spread) * earlier_scale[..., None]
        + later_sum.reshape(spread) * later_scale[..., None]
    )
    return (
        row_max,
        earlier_total * earlier_scale + later_total * later_scale,
        joined.reshape(earlier_sum.shape),
    )


def block_part(scores, live_mask, block_values):
    seq_count, heads_local, prop_count, key_count = scores.shape
    row_max = jnp.max(scores, axis=3)
    weights = jnp.where(live_mask, jnp.exp(scores - row_max[..., None]), 0.0)
    row_total = jnp.sum(weights, axis=3)
    weighted = jnp.einsum(
        "shpk,skhd->sphd",
        weights.astype(jnp.bfloat16),
        block_values,
        preferred_element_type=jnp.float32,
    )
    return (
        jnp.transpose(row_max, (0, 2, 1)),
        jnp.transpose(row_total, (0, 2, 1)),
        weighted.reshape(seq_count, prop_count, -1),
    )


def finish_rows(row_sums, inverse, query_gain, key_gain, heads_local):
    head_width = row_sums.shape[1] // 3
    head_size = head_width // heads_local
    row_count = row_sums.shape[0]
    raw_sums = row_sums * inverse[:, None]
    queries = head_norm(
        raw_sums[:, :head_width].reshape(row_count, heads_local, head_size), query_gain
    )
    keyed = head_norm(
        raw_sums[:, head_width : 2 * head_width].reshape(row_count, heads_local, head_size),
        key_gain,
    )
    return jnp.concatenate(
        [
            queries.reshape(row_count, head_width),
            keyed.reshape(row_count, head_width),
            raw_sums[:, 2 * head_width :],
        ],
        axis=1,
    ).astype(jnp.bfloat16)


def flatten_part(part_triple, rows_all):
    part_max, part_total, part_sum = part_triple
    return (
        part_max.reshape(rows_all, -1),
        part_total.reshape(rows_all, -1),
        part_sum.reshape(rows_all, -1),
    )


def shards(
    tokens,
    norm_gain,
    w_query,
    w_key,
    w_value,
    w_forget,
    forget_bias,
    query_gain,
    key_gain,
    head_gain,
    w_out,
    key_cache,
    value_cache,
    gate_cache,
    lengths,
    accepted,
    parents,
):
    seq_count, prop_count, width_in = tokens.shape
    pos_dev = key_cache.shape[1]
    heads_local = gate_cache.shape[1]
    head_width = key_cache.shape[2]
    head_size = head_width // heads_local
    rows_all = seq_count * prop_count
    full_width = w_forget.shape[0]
    kv_index = lax.axis_index("kv")
    tp_index = lax.axis_index("tp")
    flattened = tokens.reshape(rows_all, width_in).astype(jnp.float32)
    squares = jnp.sum(flattened * flattened, axis=1)
    scaled = (flattened * norm_gain).astype(jnp.bfloat16)
    w_rows = lax.dynamic_slice_in_dim(w_forget, kv_index * width_in, width_in, 0)
    gate_part = jnp.dot(scaled, w_rows, preferred_element_type=jnp.float32)
    w_joined = jnp.concatenate([w_query, w_key, w_value], axis=1)
    summed, gate_sum, square_sum = lax.psum(
        (jnp.dot(scaled, w_joined, preferred_element_type=jnp.float32), gate_part, squares), "kv"
    )
    inverse = lax.rsqrt(square_sum / full_width + EPSILON)
    joined = finish_rows(summed, inverse, query_gain, key_gain, heads_local)
    log_all = jax.nn.log_sigmoid(gate_sum * inverse[:, None] + forget_bias)
    log_own = lax.dynamic_slice_in_dim(log_all, tp_index * heads_local, heads_local, 1)
    log_own = log_own.reshape(seq_count, prop_count, heads_local)
    queries = joined[:, :head_width].reshape(seq_count, prop_count, heads_local, head_size)
    keys_new = joined[:, head_width : 2 * head_width].reshape(
        seq_count, prop_count, heads_local, head_size
    )
    values_new = joined[:, 2 * head_width :].reshape(seq_count, prop_count, heads_local, head_size)
    ancestors = ancestry(parents)
    path_sum = jnp.einsum("sij,sjh->sih", ancestors, log_own, precision=lax.Precision.HIGHEST)
    base_pos = lengths + accepted
    positions = kv_index * pos_dev + jnp.arange(pos_dev, dtype=jnp.int32)
    score_scale = head_size ** (-0.5)
    cached_keys = key_cache.reshape(seq_count, pos_dev, heads_local, head_size)
    cached_values = value_cache.reshape(seq_count, pos_dev, heads_local, head_size)
    scores = jnp.einsum("sphd,skhd->shpk", queries, cached_keys, preferred_element_type=jnp.float32)
    scores = scores * score_scale - gate_cache[:, :, None, :]
    live_mask = (positions[None, :] < base_pos[:, None])[:, None, None, :]
    scores = jnp.where(live_mask, scores, MASKED)
    local_part = block_part(scores, live_mask, cached_values)
    hit_mask = positions[None, :] == (base_pos - 1)[:, None]
    boundary_local = jnp.sum(jnp.where(hit_mask[:, None, :], gate_cache, 0.0), axis=2)
    tree_live = (ancestors > 0.5)[:, None, :, :]
    boundary = lax.psum(boundary_local, "kv")
    flat_max, flat_total, flat_sum = flatten_part(local_part, rows_all)
    got_max, got_total, got_sum = (
        lax.all_to_all(flat_max[None], "kv", split_axis=1, concat_axis=0, tiled=True),
        lax.all_to_all(flat_total[None], "kv", split_axis=1, concat_axis=0, tiled=True),
        lax.all_to_all(flat_sum[None], "kv", split_axis=1, concat_axis=0, tiled=True),
    )
    top = jnp.max(got_max, axis=0)
    factors = jnp.exp(got_max - top[None])
    own_rows = got_max.shape[1]
    summed_rows = jnp.sum(
        got_sum.reshape(got_sum.shape[0], own_rows, heads_local, head_size) * factors[..., None],
        axis=0,
    )
    merged = (top, jnp.sum(got_total * factors, axis=0), summed_rows.reshape(own_rows, head_width))
    tree_scores = jnp.einsum(
        "sphd,sjhd->shpj", queries, keys_new, preferred_element_type=jnp.float32
    )
    tree_scores = (
        tree_scores * score_scale
        - jnp.transpose(path_sum, (0, 2, 1))[:, :, None, :]
        - boundary[:, :, None, None]
    )
    tree_scores = jnp.where(tree_live, tree_scores, MASKED)
    tree_max, tree_total, tree_sum = flatten_part(
        block_part(tree_scores, tree_live, values_new), rows_all
    )
    row_lower = kv_index * own_rows
    merged = combine(
        merged,
        (
            lax.dynamic_slice_in_dim(tree_max, row_lower, own_rows, 0),
            lax.dynamic_slice_in_dim(tree_total, row_lower, own_rows, 0),
            lax.dynamic_slice_in_dim(tree_sum, row_lower, own_rows, 0),
        ),
    )
    row_max, row_total, weighted = merged
    attended = weighted.reshape(own_rows, heads_local, head_size) / row_total[..., None]
    own_normed = head_norm(attended, head_gain).astype(jnp.bfloat16).reshape(own_rows, head_width)
    normed = lax.all_gather(own_normed, "kv", axis=0, tiled=True)
    out_term = jnp.dot(normed, w_out, preferred_element_type=jnp.float32)
    layer_out = lax.psum(out_term.astype(jnp.bfloat16), "tp")
    layer_out = layer_out.reshape(seq_count, prop_count, -1)
    new_rows = jnp.concatenate(
        [
            keys_new.reshape(seq_count, prop_count, head_width),
            values_new.reshape(seq_count, prop_count, head_width),
        ],
        axis=2,
    )
    slot_index = positions[None, :, None] - base_pos[:, None, None]
    placing = slot_index == jnp.arange(prop_count, dtype=jnp.int32)[None, None, :]
    written = jnp.einsum(
        "skp,spc->skc", placing.astype(jnp.bfloat16), new_rows, preferred_element_type=jnp.float32
    ).astype(jnp.bfloat16)
    hit_rows = jnp.any(placing, axis=2)[..., None]
    new_keys = jnp.where(hit_rows, written[..., :head_width], key_cache)
    new_values = jnp.where(hit_rows, written[..., head_width:], value_cache)
    return (layer_out, new_keys, new_values, log_own)


def solution(mesh):
    placed = (
        P("dp", None, "kv"),
        P("kv"),
        P("kv", "tp"),
        P("kv", "tp"),
        P("kv", "tp"),
        P(),
        P(),
        P(),
        P(),
        P(),
        P("tp", "kv"),
        P("dp", "kv", "tp"),
        P("dp", "kv", "tp"),
        P("dp", "tp", "kv"),
        P("dp"),
        P("dp"),
        P("dp", None),
    )
    return jax.shard_map(
        shards,
        mesh=mesh,
        in_specs=placed,
        out_specs=(
            P("dp", None, "kv"),
            P("dp", "kv", "tp"),
            P("dp", "kv", "tp"),
            P("dp", None, "tp"),
        ),
        check_vma=False,
    )
```

profile of v0, /device:TPU:0, one launch (start us, length us, event | category | flops | bytes accessed | tf_op | source)
XLA Modules:
  0.0 129.3 jit_solution(6320880123169172122)
XLA Ops:
  7.2 0.9 fusion.29
  8.3 2.6 %fusion.6 = f32[64,1536]{1,0:T(8,128)} fusion(bf16[64,512]{1,0:T(8,128)(2,1)S(1)} %fusion.29, bf16[512,512]{1,0:T(8,128)(2,1)} %param.23, bf16[512,512]{1,0:T(8,128)(2,1)} %param.22, bf16[512,512]{1,0:T(8,128)(2,1)} %param.21), kind=kOutput, calls=%fused_computation.9 | convolution fusion | flops 105381888 | bytes 2031616 | tf_op jit(solution)/shard_map/dot_general | solution.py:131
  11.2 4.2 %while.11 = (s32[]{:T(128)}, f32[4,16,16]{2,1,0:T(8,128)S(1)}, s32[4,16]{1,0:T(4,128)S(1)}, f32[16,16]{1,0:T(8,128)S(1)}, s32[]{:T(128)}) while((s32[]{:T(128)}, f32[4,16,16]{2,1,0:T(8,128)S(1)}, s32[4,16]{1,0:T(4,128)S(1)}, f32[16,16]{1,0:T(8,128)S(1)}, s32[]{:T(128)}) %tuple.50), condition=%wide.region_8.9_spmd.clone, body=%wide.region_7.8_spmd.clone.sunk | while | flops 199682 | bytes 17725 | solution.py:26
  15.6 0.8 fusion.39
  16.4 20.4 %all-reduce = (f32[64]{0:T(128)S(1)}, f32[4,8]{1,0:T(4,128)S(1)}, f32[64,16]{0,1:T(8,128)S(1)}) all-reduce(f32[64]{0:T(128)S(1)} %reduce_sum.86, f32[4,8]{1,0:T(4,128)S(1)} %select_reduce_fusion, f32[64,16]{0,1:T(8,128)S(1)} %fusion.39), channel_id=1, replica_groups=mesh['dp'=4,'kv'=4,'tp'=2] {'kv'}, use_global_device_ids=true, to_apply=%region_2.0 | all-reduce | flops 1120 | bytes 8960 | tf_op jit(solution)/shard_map/psum | solution.py:130
  37.4 4.3 %copy.136 = bf16[4,512,512]{1,2,0:T(8,128)(2,1)} copy(bf16[4,512,512]{2,1,0:T(8,128)(2,1)} %param.30) | data formatting | bytes 4194304 | tf_op args[11]
  41.7 2.4 %copy.138 = bf16[4,512,512]{1,2,0:T(8,128)(2,1)} copy(bf16[4,512,512]{2,1,0:T(8,128)(2,1)S(1)} %copy-done.1) | data formatting | bytes 4194304 | tf_op args[12]
  44.3 6.7 %all-reduce.4.cloned.1.call-done = f32[64,1536]{1,0:T(8,128)} async-done(((f32[64,1536]{1,0:T(8,128)}), f32[64,1536]{1,0:T(8,128)}) %all-reduce.4.cloned.1.call-update) | async-done | bytes 393232 | tf_op jit(solution)/shard_map/psum | solution.py:130
  51.0 1.1 broadcast_multiply_fusion
  53.9 2.1 %fusion.57 = (f32[4,8,16]{2,1,0:T(8,128)S(1)}, f32[4,8,16,512]{3,2,1,0:T(8,128)S(1)}) fusion(f32[4,8,512]{2,1,0:T(8,128)S(1)} %copy-done.3, bf16[4,512,8,64]{1,3,2,0:T(8,128)(2,1)} %bitcast.48, bf16[4,16,8,64]{3,2,1,0:T(8,128)(2,1)S(1)} %reshape.230, pred[4,512]{1,0:T(4,128)(4,1)S(1)} %get-tuple-element.90), kind=kOutput, calls=%fused_computation.96 | convolution fusion | flops 34602496 | bytes 3280896 | tf_op jit(solution)/shard_map/sphd,skhd->shpk/dot_general | solution.py:150
  58.3 3.4 %all-to-all-start.2 = ((f32[4,1,128]{2,1,0:T(1,128)}), f32[4,1,128]{2,1,0:T(1,128)S(1)}, u32[]{:S(2)}, u32[]{:S(2)}) async-start(f32[4,1,128]{2,1,0:T(1,128)} %reshape.243), calls=%async_computation.2 | async-start | bytes 4096 | tf_op jit(solution)/shard_map/all_to_all | solution.py:162
  61.8 2.3 %convolution_bitcast_fusion = f32[4,16,8,64]{3,1,2,0:T(8,128)S(1)} fusion(bf16[4,512,8,64]{1,3,2,0:T(8,128)(2,1)} %bitcast.47, f32[4,8,16,512]{3,2,1,0:T(8,128)S(1)} %get-tuple-element.95, f32[4,8,16]{2,1,0:T(8,128)S(1)} %get-tuple-element.94, pred[4,512]{1,0:T(4,128)(4,1)S(1)} %get-tuple-element.90), kind=kOutput, calls=%fused_computation.21 | convolution fusion | flops 34340864 | bytes 3280896 | tf_op jit(solution)/shard_map/shpk,skhd->sphd/dot_general | solution.py:52
  64.1 3.2 %convolution_convert_fusion = bf16[4,512,1024]{2,1,0:T(8,128)(2,1)} fusion(bf16[4,16,512]{2,1,0:T(8,128)(2,1)S(1)} %bitcast.50, bf16[4,16,512]{2,1,0:T(8,128)(2,1)S(1)} %bitcast.49, s32[4,512]{1,0:T(4,128)S(1)} %broadcast_subtract_fusion), kind=kOutput, calls=%fused_computation.6 | convolution fusion | flops 69500928 | bytes 4333568 | tf_op jit(solution)/shard_map/skp,spc->skc/dot_general | solution.py:210
  68.2 0.7 reduce.4
  69.6 5.1 %all-to-all-start.1 = ((f32[4,1,128]{2,1,0:T(1,128)}), f32[4,1,128]{2,1,0:T(1,128)S(1)}, u32[]{:S(2)}, u32[]{:S(2)}) async-start(f32[4,1,128]{2,1,0:T(1,128)} %reshape.241), calls=%async_computation.1 | async-start | bytes 4096 | tf_op jit(solution)/shard_map/all_to_all | solution.py:161
  75.0 0.8 broadcast_in_dim_reshape_reshape.4
  76.6 3.6 %all-to-all-done.1 = f32[4,1,128]{2,1,0:T(1,128)S(1)} async-done(((f32[4,1,128]{2,1,0:T(1,128)}), f32[4,1,128]{2,1,0:T(1,128)S(1)}, u32[]{:S(2)}, u32[]{:S(2)}) %all-to-all-start.1) | async-done | bytes 2080 | tf_op jit(solution)/shard_map/all_to_all | solution.py:161
  80.1 3.3 %all-to-all-start = ((f32[1,64,512]{2,0,1:T(1,128)}), f32[1,64,512]{2,0,1:T(1,128)S(1)}, u32[]{:S(2)}, u32[]{:S(2)}) async-start(f32[1,64,512]{2,0,1:T(1,128)} %broadcast_in_dim_reshape_reshape.4), calls=%async_computation | async-start | bytes 262144 | tf_op jit(solution)/shard_map/all_to_all | solution.py:163
  85.2 4.2 %all-to-all-done = f32[1,64,512]{2,0,1:T(1,128)S(1)} async-done(((f32[1,64,512]{2,0,1:T(1,128)}), f32[1,64,512]{2,0,1:T(1,128)S(1)}, u32[]{:S(2)}, u32[]{:S(2)}) %all-to-all-start) | async-done | bytes 131104 | tf_op jit(solution)/shard_map/all_to_all | solution.py:163
  90.1 13.1 %all_gather.3 = bf16[64,512]{1,0:T(8,128)(2,1)S(1)} all-gather(bf16[16,512]{1,0:T(8,128)(2,1)S(1)} %multiply_convert_fusion.2), channel_id=1, replica_groups=mesh['dp'=4,'kv'=4,'tp'=2] {'kv'}, dimensions={0}, use_global_device_ids=true | all-gather | bytes 81920 | tf_op jit(solution)/shard_map/all_gather | solution.py:197
  103.2 0.8 convolution_convert_fusion.1
  104.1 4.4 %slice_select_fusion = (bf16[4,512,512]{2,1,0:T(8,128)(2,1)}, bf16[4,512,512]{2,1,0:T(8,128)(2,1)}) fusion(bf16[4,512,512]{2,1,0:T(8,128)(2,1)S(1)} %copy-done.2, bf16[4,512,1024]{2,1,0:T(8,128)(2,1)} %convolution_convert_fusion, pred[4,512]{1,0:T(4,128)(4,1)S(1)} %fusion.32, bf16[4,512,512]{2,1,0:T(8,128)(2,1)} %param.30), kind=kLoop, calls=%fused_computation.7 | loop fusion | flops 2097152 | bytes 12584960 | tf_op jit(solution)/shard_map/jit(_where)/select_n | solution.py:215
  108.5 12.4 %all-reduce.6.cloned.1.call-done = bf16[4,16,512]{2,1,0:T(8,128)(2,1)} async-done(((bf16[4,16,512]{2,1,0:T(8,128)(2,1)}), bf16[4,16,512]{2,1,0:T(8,128)(2,1)}) %all-reduce.6.cloned.1.call-update) | async-done | bytes 65552 | tf_op jit(solution)/shard_map/psum | solution.py:199
  121.0 1.5 %copy.192 = bf16[4,16,512]{2,1,0:T(8,128)(2,1)} copy(bf16[4,16,512]{2,1,0:T(8,128)(2,1)} %all-reduce.6.cloned.1.call-done) | data formatting | bytes 131072
  (146 shorter events, 14.0 us)
Async XLA Ops:
  7.2 96.0 %copy-start = (bf16[512,512]{1,0:T(8,128)(2,1)S(1)}, bf16[512,512]{1,0:T(8,128)(2,1)}, u32[]{:S(2)}) copy-start(bf16[512,512]{1,0:T(8,128)(2,1)} %param.29) | copy-start | bytes 1572868
  7.2 43.8 %all-reduce.4.cloned.1.call-start = ((), (), s32[]{:S(2)}) async-start(), calls=%async_computation.3 | async-start | bytes 786432 | tf_op jit(solution)/shard_map/psum | solution.py:130
  8.1 2.7 %copy-start.4 = (bf16[4,16,512]{2,1,0:T(8,128)(2,1)S(1)}, bf16[4,16,512]{2,1,0:T(8,128)(2,1)}, u32[]{:S(2)}) copy-start(bf16[4,16,512]{2,1,0:T(8,128)(2,1)} %param.19) | copy-start | bytes 196612
  8.2 2.9 %copy-start.11 = (s32[4]{0:T(128)S(1)}, s32[4]{0:T(128)}, u32[]{:S(2)}) copy-start(s32[4]{0:T(128)} %param.33) | copy-start | bytes 52
  8.2 2.9 %copy-start.12 = (s32[4]{0:T(128)S(1)}, s32[4]{0:T(128)}, u32[]{:S(2)}) copy-start(s32[4]{0:T(128)} %param.34) | copy-start | bytes 52
  8.2 3.0 %copy-start.6 = (s32[4,16]{1,0:T(4,128)S(1)}, s32[4,16]{1,0:T(4,128)}, u32[]{:S(2)}) copy-start(s32[4,16]{1,0:T(4,128)} %param.35) | copy-start | bytes 772
  8.2 7.3 %copy-start.3 = (f32[4,8,512]{2,1,0:T(8,128)S(1)}, f32[4,8,512]{2,1,0:T(8,128)}, u32[]{:S(2)}) copy-start(f32[4,8,512]{2,1,0:T(8,128)} %param.32) | copy-start | bytes 196612
  8.2 28.7 %copy-start.7 = (f32[16]{0:T(128)S(1)}, f32[16]{0:T(128)}, u32[]{:S(2)}) copy-start(f32[16]{0:T(128)} %param.25) | copy-start | bytes 196
  8.2 28.8 %copy-start.8 = (f32[64]{0:T(128)S(1)}, f32[64]{0:T(128)}, u32[]{:S(2)}) copy-start(f32[64]{0:T(128)} %param.26) | copy-start | bytes 772
  8.2 28.8 %copy-start.9 = (f32[64]{0:T(128)S(1)}, f32[64]{0:T(128)}, u32[]{:S(2)}) copy-start(f32[64]{0:T(128)} %param.27) | copy-start | bytes 772
  8.2 28.9 %copy-start.10 = (f32[64]{0:T(128)S(1)}, f32[64]{0:T(128)}, u32[]{:S(2)}) copy-start(f32[64]{0:T(128)} %param.28) | copy-start | bytes 772
  37.4 6.7 %copy-start.5 = (f32[4,16,8]{1,2,0:T(8,128)}, f32[4,16,8]{1,2,0:T(8,128)S(1)}, u32[]{:S(2)}) copy-start(f32[4,16,8]{1,2,0:T(8,128)S(1)} %copy.148) | copy-start | bytes 6148
  37.4 4.3 %copy-start.1 = (bf16[4,512,512]{2,1,0:T(8,128)(2,1)S(1)}, bf16[4,512,512]{2,1,0:T(8,128)(2,1)}, u32[]{:S(2)}) copy-start(bf16[4,512,512]{2,1,0:T(8,128)(2,1)} %param.31) | copy-start | bytes 6291460
  58.3 11.2 %all-to-all-start.2 = ((f32[4,1,128]{2,1,0:T(1,128)}), f32[4,1,128]{2,1,0:T(1,128)S(1)}, u32[]{:S(2)}, u32[]{:S(2)}) async-start(f32[4,1,128]{2,1,0:T(1,128)} %reshape.243), calls=%async_computation.2 | async-start | bytes 4096 | tf_op jit(solution)/shard_map/all_to_all | solution.py:162
  69.6 10.6 %all-to-all-start.1 = ((f32[4,1,128]{2,1,0:T(1,128)}), f32[4,1,128]{2,1,0:T(1,128)S(1)}, u32[]{:S(2)}, u32[]{:S(2)}) async-start(f32[4,1,128]{2,1,0:T(1,128)} %reshape.241), calls=%async_computation.1 | async-start | bytes 4096 | tf_op jit(solution)/shard_map/all_to_all | solution.py:161
  75.0 29.1 %copy-start.2 = (bf16[4,512,512]{2,1,0:T(8,128)(2,1)S(1)}, bf16[4,512,512]{2,1,0:T(8,128)(2,1)}, u32[]{:S(2)}) copy-start(bf16[4,512,512]{2,1,0:T(8,128)(2,1)} %param.31) | copy-start | bytes 6291460
  80.1 9.2 %all-to-all-start = ((f32[1,64,512]{2,0,1:T(1,128)}), f32[1,64,512]{2,0,1:T(1,128)S(1)}, u32[]{:S(2)}, u32[]{:S(2)}) async-start(f32[1,64,512]{2,0,1:T(1,128)} %broadcast_in_dim_reshape_reshape.4), calls=%async_computation | async-start | bytes 262144 | tf_op jit(solution)/shard_map/all_to_all | solution.py:163
  83.5 37.5 %all-reduce.6.cloned.1.call-start = ((), (), s32[]{:S(2)}) async-start(), calls=%async_computation.4 | async-start | bytes 131072 | tf_op jit(solution)/shard_map/psum | solution.py:199
Sparse Core Ops, SparseCore 0:
  11.0 39.9 all-reduce.3
  104.2 16.7 all-reduce.5
where the time goes:
time: 130 us; the launch traced here: 129 us
  blocking collectives  33.6 us (26%)
  waiting for transfers between devices  27 us (21%)
  matrix products  16.2 us (12%)
  local copies, waits for them, and re-layouts  14.8 us (11%)
  between operations  14.5 us (11%)
  starting transfers between devices  11.9 us (9%)
  other arithmetic  10.9 us (8%)
    psum x1, blocking collectives, shards(): lax.psum((jnp.dot(scaled, w_joined, preferred_element_type=jnp.float32),...  20.4 us
    all_gather x1, blocking collectives, shards(): normed = lax.all_gather(own_normed, 'kv', axis=0, tiled=True)  13.1 us
    psum x1, waiting for transfers between devices, shards(): layer_out = lax.psum(out_term.astype(jnp.bfloat16), 'tp')  12.4 us
    unnamed x34, local copies, waits for them, and re-layouts  10.3 us
    psum x1, waiting for transfers between devices, shards(): lax.psum((jnp.dot(scaled, w_joined, preferred_element_type=jnp.float32),...  6.72 us
    all_to_all x1, starting transfers between devices, shards(): lax.all_to_all(flat_max[None], 'kv', split_axis=1, concat_axis=0, tiled=T...  5.09 us
    select_n x1, other arithmetic, shards(): new_values = jnp.where(hit_rows, written[..., head_width:], value_cache)  4.45 us
    all_to_all x1, waiting for transfers between devices, shards(): lax.all_to_all(flat_sum[None], 'kv', split_axis=1, concat_axis=0, tiled=T...  4.2 us
  transfers between devices with their start and end apart: 5, of which 4 were waited for; matrix products, arithmetic and copies ran while one was open for 22% of the time, Pallas kernels for 0%

commit v1 on v0

--- a/solution.py
+++ b/solution.py
@@ -196,7 +196,7 @@
     own_normed = head_norm(attended, head_gain).astype(jnp.bfloat16).reshape(own_rows, head_width)
     normed = lax.all_gather(own_normed, "kv", axis=0, tiled=True)
     out_term = jnp.dot(normed, w_out, preferred_element_type=jnp.float32)
-    layer_out = lax.psum(out_term.astype(jnp.bfloat16), "tp")
+    layer_out = jnp.sum(lax.all_gather(out_term.astype(jnp.bfloat16), "tp"), axis=0)
     layer_out = layer_out.reshape(seq_count, prop_count, -1)
     new_rows = jnp.concatenate(
         [

time: 130 us -> 115 us (0.88)
  waiting for transfers between devices: 27 us -> 14.5 us
  matrix products: 16.2 us -> 13.6 us
  blocking collectives: 33.6 us -> 35.5 us
    psum x1 -> x0, waiting for transfers between devices: 12.4 us -> none  [shards(): layer_out = lax.psum(out_term.astype(jnp.bfloat16), 'tp')]
    select_n x1, other arithmetic: 4.45 us -> 2.33 us  [shards(): new_values = jnp.where(hit_rows, written[..., head_width:], value_cache)]
    dot_general x1, matrix products: 3.24 us -> 1.31 us  [shards(): jnp.einsum('skp,spc->skc', placing.astype(jnp.bfloat16), new_rows, prefer...]
    all_gather x0 -> x1, blocking collectives: none -> 1.9 us  [shards(): lax.all_gather(out_term.astype(jnp.bfloat16), 'tp')]
    unnamed x34 -> x35, local copies, waits for them, and re-layouts: 10.3 us -> 9.8 us
  transfers between devices with their start and end apart: 5 -> 4, of which waited for: 4 -> 3; matrix products, arithmetic and copies ran while one was open for 22% -> 21% of each run, Pallas kernels for 0% -> 0%
where the time goes in v1:
time: 115 us; the launch traced here: 114 us
  blocking collectives  35.5 us (31%)
  waiting for transfers between devices  14.5 us (13%)
  between operations  14.5 us (13%)
  local copies, waits for them, and re-layouts  14.3 us (12%)
  matrix products  13.6 us (12%)
  starting transfers between devices  11.9 us (10%)
  other arithmetic  9.68 us (8%)
    psum x1, blocking collectives, shards(): lax.psum((jnp.dot(scaled, w_joined, preferred_element_type=jnp.float32),...  20.4 us
    all_gather x1, blocking collectives, shards(): normed = lax.all_gather(own_normed, 'kv', axis=0, tiled=True)  13.1 us
    unnamed x35, local copies, waits for them, and re-layouts  9.8 us
    psum x1, waiting for transfers between devices, shards(): lax.psum((jnp.dot(scaled, w_joined, preferred_element_type=jnp.float32),...  6.72 us
    all_to_all x1, starting transfers between devices, shards(): lax.all_to_all(flat_max[None], 'kv', split_axis=1, concat_axis=0, tiled=T...  5.09 us
    all_to_all x1, waiting for transfers between devices, shards(): lax.all_to_all(flat_sum[None], 'kv', split_axis=1, concat_axis=0, tiled=T...  4.19 us
    dot_general x16, matrix products, extend(): jnp.einsum('sij,sjk->sik', step_matrix, ancestors, precision=lax.Precisio...  3.67 us
    all_to_all x1, waiting for transfers between devices, shards(): lax.all_to_all(flat_max[None], 'kv', split_axis=1, concat_axis=0, tiled=T...  3.62 us
  transfers between devices with their start and end apart: 4, of which 3 were waited for; matrix products, arithmetic and copies ran while one was open for 21% of the time, Pallas kernels for 0%

profile of v1, /device:TPU:0, one launch (start us, length us, event | category | flops | bytes accessed | tf_op | source)
XLA Modules:
  0.0 114.4 jit_solution(15848074861492798127)
XLA Ops:
  7.2 0.9 fusion.29
  8.3 2.6 %fusion.6 = f32[64,1536]{1,0:T(8,128)} fusion(bf16[64,512]{1,0:T(8,128)(2,1)S(1)} %fusion.29, bf16[512,512]{1,0:T(8,128)(2,1)} %param.23, bf16[512,512]{1,0:T(8,128)(2,1)} %param.22, bf16[512,512]{1,0:T(8,128)(2,1)} %param.21), kind=kOutput, calls=%fused_computation.9 | convolution fusion | flops 105381888 | bytes 2031616 | tf_op jit(solution)/shard_map/dot_general | solution.py:131
  11.2 4.2 %while.11 = (s32[]{:T(128)}, f32[4,16,16]{2,1,0:T(8,128)S(1)}, s32[4,16]{1,0:T(4,128)S(1)}, f32[16,16]{1,0:T(8,128)S(1)}, s32[]{:T(128)}) while((s32[]{:T(128)}, f32[4,16,16]{2,1,0:T(8,128)S(1)}, s32[4,16]{1,0:T(4,128)S(1)}, f32[16,16]{1,0:T(8,128)S(1)}, s32[]{:T(128)}) %tuple.47), condition=%wide.region_8.9_spmd.clone, body=%wide.region_7.8_spmd.clone.sunk | while | flops 199682 | bytes 17725 | solution.py:26
  15.6 0.8 fusion.39
  16.4 20.4 %all-reduce = (f32[64]{0:T(128)S(1)}, f32[4,8]{1,0:T(4,128)S(1)}, f32[64,16]{0,1:T(8,128)S(1)}) all-reduce(f32[64]{0:T(128)S(1)} %reduce_sum.98, f32[4,8]{1,0:T(4,128)S(1)} %select_reduce_fusion, f32[64,16]{0,1:T(8,128)S(1)} %fusion.39), channel_id=1, replica_groups=mesh['dp'=4,'kv'=4,'tp'=2] {'kv'}, use_global_device_ids=true, to_apply=%region_2.0 | all-reduce | flops 1120 | bytes 8960 | tf_op jit(solution)/shard_map/psum | solution.py:130
  37.4 4.3 %copy.136 = bf16[4,512,512]{1,2,0:T(8,128)(2,1)} copy(bf16[4,512,512]{2,1,0:T(8,128)(2,1)} %param.30) | data formatting | bytes 4194304 | tf_op args[11]
  41.7 2.4 %copy.138 = bf16[4,512,512]{1,2,0:T(8,128)(2,1)} copy(bf16[4,512,512]{2,1,0:T(8,128)(2,1)S(1)} %copy-done.1) | data formatting | bytes 4194304 | tf_op args[12]
  44.3 6.7 %all-reduce.3.cloned.1.call-done = f32[64,1536]{1,0:T(8,128)} async-done(((f32[64,1536]{1,0:T(8,128)}), f32[64,1536]{1,0:T(8,128)}) %all-reduce.3.cloned.1.call-update) | async-done | bytes 393232 | tf_op jit(solution)/shard_map/psum | solution.py:130
  51.0 1.1 broadcast_multiply_fusion
  53.9 2.1 %fusion.57 = (f32[4,8,16]{2,1,0:T(8,128)S(1)}, f32[4,8,16,512]{3,2,1,0:T(8,128)S(1)}) fusion(f32[4,8,512]{2,1,0:T(8,128)S(1)} %copy-done.4, bf16[4,512,8,64]{1,3,2,0:T(8,128)(2,1)} %bitcast.49, bf16[4,16,8,64]{3,2,1,0:T(8,128)(2,1)S(1)} %reshape.230, pred[4,512]{1,0:T(4,128)(4,1)S(1)} %get-tuple-element.90), kind=kOutput, calls=%fused_computation.96 | convolution fusion | flops 34602496 | bytes 3280896 | tf_op jit(solution)/shard_map/sphd,skhd->shpk/dot_general | solution.py:150
  57.0 0.8 reduce.3
  58.5 3.4 %all-to-all-start.2 = ((f32[4,1,128]{2,1,0:T(1,128)}), f32[4,1,128]{2,1,0:T(1,128)S(1)}, u32[]{:S(2)}, u32[]{:S(2)}) async-start(f32[4,1,128]{2,1,0:T(1,128)} %reshape.244), calls=%async_computation.2 | async-start | bytes 4096 | tf_op jit(solution)/shard_map/all_to_all | solution.py:162
  61.9 2.3 %convolution_bitcast_fusion = f32[4,16,8,64]{3,1,2,0:T(8,128)S(1)} fusion(bf16[4,512,8,64]{1,3,2,0:T(8,128)(2,1)} %bitcast.48, f32[4,8,16,512]{3,2,1,0:T(8,128)S(1)} %get-tuple-element.95, f32[4,8,16]{2,1,0:T(8,128)S(1)} %get-tuple-element.94, pred[4,512]{1,0:T(4,128)(4,1)S(1)} %get-tuple-element.90), kind=kOutput, calls=%fused_computation.21 | convolution fusion | flops 34340864 | bytes 3280896 | tf_op jit(solution)/shard_map/shpk,skhd->sphd/dot_general | solution.py:52
  64.2 1.3 %convolution_convert_fusion = bf16[4,512,1024]{2,1,0:T(8,128)(2,1)S(1)} fusion(bf16[4,16,512]{2,1,0:T(8,128)(2,1)S(1)} %bitcast.51, bf16[4,16,512]{2,1,0:T(8,128)(2,1)S(1)} %bitcast.50, s32[4,512]{1,0:T(4,128)S(1)} %broadcast_subtract_fusion), kind=kOutput, calls=%fused_computation.6 | convolution fusion | flops 69500928 | bytes 4333568 | tf_op jit(solution)/shard_map/skp,spc->skc/dot_general | solution.py:210
  66.4 2.3 %slice_select_fusion = (bf16[4,512,512]{2,1,0:T(8,128)(2,1)}, bf16[4,512,512]{2,1,0:T(8,128)(2,1)}) fusion(bf16[4,512,512]{2,1,0:T(8,128)(2,1)S(1)} %copy-done.2, bf16[4,512,1024]{2,1,0:T(8,128)(2,1)S(1)} %convolution_convert_fusion, pred[4,512]{1,0:T(4,128)(4,1)S(1)} %fusion.32, bf16[4,512,512]{2,1,0:T(8,128)(2,1)S(1)} %copy-done.3), kind=kLoop, calls=%fused_computation.7 | loop fusion | flops 2097152 | bytes 12584960 | tf_op jit(solution)/shard_map/jit(_where)/select_n | solution.py:215
  69.6 0.8 reduce.5
  71.1 5.1 %all-to-all-start.1 = ((f32[4,1,128]{2,1,0:T(1,128)}), f32[4,1,128]{2,1,0:T(1,128)S(1)}, u32[]{:S(2)}, u32[]{:S(2)}) async-start(f32[4,1,128]{2,1,0:T(1,128)} %reshape.242), calls=%async_computation.1 | async-start | bytes 4096 | tf_op jit(solution)/shard_map/all_to_all | solution.py:161
  76.5 0.8 broadcast_in_dim_reshape_reshape.4
  78.1 3.6 %all-to-all-done.1 = f32[4,1,128]{2,1,0:T(1,128)S(1)} async-done(((f32[4,1,128]{2,1,0:T(1,128)}), f32[4,1,128]{2,1,0:T(1,128)S(1)}, u32[]{:S(2)}, u32[]{:S(2)}) %all-to-all-start.1) | async-done | bytes 2080 | tf_op jit(solution)/shard_map/all_to_all | solution.py:161
  81.7 3.3 %all-to-all-start = ((f32[1,64,512]{2,0,1:T(1,128)}), f32[1,64,512]{2,0,1:T(1,128)S(1)}, u32[]{:S(2)}, u32[]{:S(2)}) async-start(f32[1,64,512]{2,0,1:T(1,128)} %broadcast_in_dim_reshape_reshape.4), calls=%async_computation | async-start | bytes 262144 | tf_op jit(solution)/shard_map/all_to_all | solution.py:163
  85.1 0.7 reduce.6
  86.8 4.2 %all-to-all-done = f32[1,64,512]{2,0,1:T(1,128)S(1)} async-done(((f32[1,64,512]{2,0,1:T(1,128)}), f32[1,64,512]{2,0,1:T(1,128)S(1)}, u32[]{:S(2)}, u32[]{:S(2)}) %all-to-all-start) | async-done | bytes 131104 | tf_op jit(solution)/shard_map/all_to_all | solution.py:163
  91.6 13.1 %all_gather.9 = bf16[64,512]{1,0:T(8,128)(2,1)S(1)} all-gather(bf16[16,512]{1,0:T(8,128)(2,1)S(1)} %multiply_convert_fusion.2), channel_id=1, replica_groups=mesh['dp'=4,'kv'=4,'tp'=2] {'kv'}, dimensions={0}, use_global_device_ids=true | all-gather | bytes 81920 | tf_op jit(solution)/shard_map/all_gather | solution.py:197
  105.0 1.9 %all-gather = bf16[128,512]{1,0:T(8,128)(2,1)S(1)} all-gather(bf16[64,512]{1,0:T(8,128)(2,1)S(1)} %convolution_convert_fusion.1), channel_id=2, replica_groups=mesh['dp'=4,'kv'=4,'tp'=2] {'tp'}, dimensions={0}, use_global_device_ids=true | all-gather | bytes 196608 | tf_op jit(solution)/shard_map/all_gather | solution.py:199
  (146 shorter events, 14.5 us)
Async XLA Ops:
  7.2 97.6 %copy-start = (bf16[512,512]{1,0:T(8,128)(2,1)S(1)}, bf16[512,512]{1,0:T(8,128)(2,1)}, u32[]{:S(2)}) copy-start(bf16[512,512]{1,0:T(8,128)(2,1)} %param.29) | copy-start | bytes 1572868
  7.2 43.8 %all-reduce.3.cloned.1.call-start = ((), (), s32[]{:S(2)}) async-start(), calls=%async_computation.3 | async-start | bytes 786432 | tf_op jit(solution)/shard_map/psum | solution.py:130
  8.1 2.7 %copy-start.5 = (bf16[4,16,512]{2,1,0:T(8,128)(2,1)S(1)}, bf16[4,16,512]{2,1,0:T(8,128)(2,1)}, u32[]{:S(2)}) copy-start(bf16[4,16,512]{2,1,0:T(8,128)(2,1)} %param.19) | copy-start | bytes 196612
  8.2 2.9 %copy-start.12 = (s32[4]{0:T(128)S(1)}, s32[4]{0:T(128)}, u32[]{:S(2)}) copy-start(s32[4]{0:T(128)} %param.33) | copy-start | bytes 52
  8.2 2.9 %copy-start.13 = (s32[4]{0:T(128)S(1)}, s32[4]{0:T(128)}, u32[]{:S(2)}) copy-start(s32[4]{0:T(128)} %param.34) | copy-start | bytes 52
  8.2 3.0 %copy-start.7 = (s32[4,16]{1,0:T(4,128)S(1)}, s32[4,16]{1,0:T(4,128)}, u32[]{:S(2)}) copy-start(s32[4,16]{1,0:T(4,128)} %param.35) | copy-start | bytes 772
  8.2 7.3 %copy-start.4 = (f32[4,8,512]{2,1,0:T(8,128)S(1)}, f32[4,8,512]{2,1,0:T(8,128)}, u32[]{:S(2)}) copy-start(f32[4,8,512]{2,1,0:T(8,128)} %param.32) | copy-start | bytes 196612
  8.2 28.7 %copy-start.8 = (f32[16]{0:T(128)S(1)}, f32[16]{0:T(128)}, u32[]{:S(2)}) copy-start(f32[16]{0:T(128)} %param.25) | copy-start | bytes 196
  8.2 28.8 %copy-start.9 = (f32[64]{0:T(128)S(1)}, f32[64]{0:T(128)}, u32[]{:S(2)}) copy-start(f32[64]{0:T(128)} %param.26) | copy-start | bytes 772
  8.2 28.8 %copy-start.10 = (f32[64]{0:T(128)S(1)}, f32[64]{0:T(128)}, u32[]{:S(2)}) copy-start(f32[64]{0:T(128)} %param.27) | copy-start | bytes 772
  8.2 28.9 %copy-start.11 = (f32[64]{0:T(128)S(1)}, f32[64]{0:T(128)}, u32[]{:S(2)}) copy-start(f32[64]{0:T(128)} %param.28) | copy-start | bytes 772
  37.4 6.7 %copy-start.6 = (f32[4,16,8]{1,2,0:T(8,128)}, f32[4,16,8]{1,2,0:T(8,128)S(1)}, u32[]{:S(2)}) copy-start(f32[4,16,8]{1,2,0:T(8,128)S(1)} %copy.148) | copy-start | bytes 6148
  37.4 4.3 %copy-start.1 = (bf16[4,512,512]{2,1,0:T(8,128)(2,1)S(1)}, bf16[4,512,512]{2,1,0:T(8,128)(2,1)}, u32[]{:S(2)}) copy-start(bf16[4,512,512]{2,1,0:T(8,128)(2,1)} %param.31) | copy-start | bytes 6291460
  58.5 12.6 %all-to-all-start.2 = ((f32[4,1,128]{2,1,0:T(1,128)}), f32[4,1,128]{2,1,0:T(1,128)S(1)}, u32[]{:S(2)}, u32[]{:S(2)}) async-start(f32[4,1,128]{2,1,0:T(1,128)} %reshape.244), calls=%async_computation.2 | async-start | bytes 4096 | tf_op jit(solution)/shard_map/all_to_all | solution.py:162
  64.2 1.6 %copy-start.2 = (bf16[4,512,512]{2,1,0:T(8,128)(2,1)S(1)}, bf16[4,512,512]{2,1,0:T(8,128)(2,1)}, u32[]{:S(2)}) copy-start(bf16[4,512,512]{2,1,0:T(8,128)(2,1)} %param.31) | copy-start | bytes 6291460
  64.2 2.2 %copy-start.3 = (bf16[4,512,512]{2,1,0:T(8,128)(2,1)S(1)}, bf16[4,512,512]{2,1,0:T(8,128)(2,1)}, u32[]{:S(2)}) copy-start(bf16[4,512,512]{2,1,0:T(8,128)(2,1)} %param.30) | copy-start | bytes 6291460
  71.1 10.7 %all-to-all-start.1 = ((f32[4,1,128]{2,1,0:T(1,128)}), f32[4,1,128]{2,1,0:T(1,128)S(1)}, u32[]{:S(2)}, u32[]{:S(2)}) async-start(f32[4,1,128]{2,1,0:T(1,128)} %reshape.242), calls=%async_computation.1 | async-start | bytes 4096 | tf_op jit(solution)/shard_map/all_to_all | solution.py:161
  81.7 9.2 %all-to-all-start = ((f32[1,64,512]{2,0,1:T(1,128)}), f32[1,64,512]{2,0,1:T(1,128)S(1)}, u32[]{:S(2)}, u32[]{:S(2)}) async-start(f32[1,64,512]{2,0,1:T(1,128)} %broadcast_in_dim_reshape_reshape.4), calls=%async_computation | async-start | bytes 262144 | tf_op jit(solution)/shard_map/all_to_all | solution.py:163
Sparse Core Ops, SparseCore 0:
  11.0 39.9 all-reduce.2
